TPU v7x, 128 devices: a whole 4x4x4 slice. The times are simulated.
128 devices in a mesh: fs: 16 (over z, y), tp: 8 (over x, core).
Axes of the slice: x: 4, y: 4, z: 4, core: 2. Of those that a mesh axis runs over, the one named last changes fastest.
Arguments:
- normed_input: bfloat16 [24576, 2048], P(('fs', 'tp')), may hold values from -6 to 6
- pre_act: bfloat16 [24576, 8192], P('fs', 'tp'), may hold values from -6 to 6
- out_grad: bfloat16 [24576, 2048], P(('fs', 'tp')), may hold values from -24 to 24
- up_weight: bfloat16 [2048, 8192], P('fs', 'tp'), may hold values from -0.125 to 0.125
- down_weight: bfloat16 [8192, 2048], P('tp', 'fs'), may hold values from -0.0625 to 0.0625
Outputs:
- input_grad: bfloat16 [24576, 2048], P(('fs', 'tp'))
- up_grad: float32 [2048, 8192], P('fs', 'tp')
- down_grad: float32 [8192, 2048], P('tp', 'fs')
All inputs are finite; a program needn't handle non-finite values.
Results may differ from a plain program's by a relative error of at most 0.014.
Values may be sent and summed in bfloat16 or wider, within the bound.
A program may use at most 128 MiB of HBM per device.

v0:
```python
import jax
import jax.numpy as jnp
from jax import lax
from jax.sharding import PartitionSpec as P


def sent_together(arrays, axis, dim, along):
    ends, at = ([], 0)
    for a in arrays[:-1]:
        at += a.shape[along]
        ends.append(at)
    both = jnp.concatenate(arrays, axis=along)
    return tuple(jnp.split(lax.all_gather(both, axis, axis=dim, tiled=True), ends, axis=along))


def cut_along(x, dim, count):
    before, after = (x.shape[:dim], x.shape[dim + 1 :])
    return jnp.moveaxis(x.reshape(*before, count, -1, *after), dim, 0)


def sum_at_owner(x, axis, dim):
    tiles = cut_along(x, dim, lax.axis_size(axis))
    arrived = lax.all_to_all(tiles, axis, split_axis=0, concat_axis=0, tiled=True)
    return arrived.astype(jnp.float32).sum(axis=0)


def local(normed_input, pre_act, out_grad, up_weight, down_weight):
    rows_all, grad_rows = sent_together((normed_input, out_grad), "tp", 0, 1)
    active = jnp.maximum(pre_act.astype(jnp.float32), 0.0)
    hidden = (active * active).astype(jnp.bfloat16)
    width = pre_act.shape[1]
    columns = grad_rows
    hidden_grad = jnp.dot(
        columns,
        lax.all_gather(down_weight, "fs", axis=1, tiled=True).T,
        preferred_element_type=jnp.float32,
    )
    pre_grad = (2.0 * active * hidden_grad).astype(jnp.bfloat16)
    partial_value = jnp.dot(
        pre_grad,
        lax.all_gather(up_weight, "fs", axis=0, tiled=True).T,
        preferred_element_type=jnp.float32,
    )
    rounded = lax.optimization_barrier(partial_value.astype(jnp.bfloat16))
    summed = sum_at_owner(rounded.astype(jnp.float32).astype(jnp.bfloat16), "tp", 0)
    input_grad = summed.astype(jnp.bfloat16)
    columns = rows_all
    both = lax.psum_scatter(
        jnp.concatenate(
            [
                jnp.dot(columns.T, pre_grad, preferred_element_type=jnp.float32),
                jnp.dot(grad_rows.T, hidden, preferred_element_type=jnp.float32),
            ],
            axis=1,
        ).astype(jnp.bfloat16),
        "fs",
        scatter_dimension=0,
        tiled=True,
    ).astype(jnp.float32)
    up_grad = both[:, :width]
    down_grad = both[:, width:].T
    up_grad, down_grad = (up_grad, down_grad)
    return (input_grad, up_grad, down_grad)


def solution(mesh):
    placed = (
        P(("fs", "tp"), None),
        P("fs", "tp"),
        P(("fs", "tp"), None),
        P("fs", "tp"),
        P("tp", "fs"),
    )
    return jax.shard_map(
        local,
        mesh=mesh,
        in_specs=placed,
        out_specs=(P(("fs", "tp"), None), P("fs", "tp"), P("tp", "fs")),
        check_vma=False,
    )
```

profile of v0, /device:TPU:1, one launch (start us, length us, event | category | flops | bytes accessed | tf_op | source)
XLA Modules:
  0.0 293.3 jit_solution(11470290909760394026)
XLA Ops:
  7.2 0.0 all-gather.4.cloned.1.call-start
  7.2 2.7 pad_maximum_fusion.1
  9.9 0.0 all-gather.4.cloned.1.call-update
  9.9 0.0 all-gather.6.cloned.1.call-start
  10.0 0.7 all-gather.6.cloned.1.call-update
  10.7 0.0 all-gather.8.cloned.1.call-start
  10.7 0.7 all-gather.8.cloned.1.call-update
  11.4 0.0 copy-start.1
  11.4 0.0 reduce-scatter.4.cloned.1.call-start
  11.5 69.5 %all-gather.4.cloned.1.call-done = bf16[1536,4096]{1,0:T(8,128)(2,1)} async-done(((bf16[192,4096]{1,0:T(8,128)(2,1)}), bf16[1536,4096]{1,0:T(8,128)(2,1)}) %all-gather.4.cloned.1.call-update) | async-done | bytes 12582928 | tf_op jit(solution)/shard_map/all_gather | solution.py:13
  80.9 11.6 %fusion.8 = bf16[2048,1024]{0,1:T(8,128)(2,1)} fusion(bf16[1536,4096]{1,0:T(8,128)(2,1)} %all-gather.4.cloned.1.call-done, bf16[1536,1024]{1,0:T(8,128)(2,1)} %param.6), kind=kOutput, calls=%fused_computation.11 | convolution fusion | flops 6450839552 | bytes 13631488 | tf_op jit(solution)/shard_map/dot_general | solution.py:52
  92.6 46.1 %all-gather.6.cloned.1.call-done = bf16[1024,2048]{1,0:T(8,128)(2,1)} async-done(((bf16[1024,128]{1,0:T(8,128)(2,1)}), bf16[1024,2048]{1,0:T(8,128)(2,1)}) %all-gather.6.cloned.1.call-update) | async-done | bytes 4194320 | tf_op jit(solution)/shard_map/all_gather | solution.py:35
  138.7 0.0 copy-done.1
  138.7 0.0 copy-start
  138.7 10.3 %multiply_convert_fusion.1 = bf16[1536,1024]{1,0:T(8,128)(2,1)S(1)} fusion(bf16[1536,1024]{1,0:T(8,128)(2,1)S(1)} %copy-done.1, bf16[1024,2048]{1,0:T(8,128)(2,1)} %all-gather.6.cloned.1.call-done, bf16[1536,4096]{1,0:T(8,128)(2,1)} %all-gather.4.cloned.1.call-done), kind=kOutput, calls=%fused_computation.5 | convolution fusion | flops 6450315264 | bytes 16777216 | tf_op jit(solution)/shard_map/dot_general | solution.py:33
  149.0 0.0 copy-start.2
  149.0 1.7 copy-done.2
  150.7 0.0 copy-done
  150.7 8.4 %fusion.11 = bf16[2048,1024]{0,1:T(8,128)(2,1)} fusion(bf16[1536,1024]{1,0:T(8,128)(2,1)S(1)} %multiply_convert_fusion.1, bf16[1536,4096]{1,0:T(8,128)(2,1)S(1)} %copy-done), kind=kOutput, calls=%fused_computation.12 | convolution fusion | flops 6444548096 | bytes 13631488 | tf_op jit(solution)/shard_map/dot_general | solution.py:51
  159.1 8.4 %pad_maximum_fusion = bf16[2048,2048]{0,1:T(8,128)(2,1)} fusion(bf16[2048,1024]{0,1:T(8,128)(2,1)} %fusion.8, bf16[2048,1024]{0,1:T(8,128)(2,1)} %fusion.11), kind=kLoop, calls=%fused_computation | loop fusion | flops 16777216 | bytes 16777216 | tf_op jit(solution)/shard_map/concatenate | solution.py:49
  167.5 11.9 %copy.10 = bf16[2048,2048]{1,0:T(8,128)(2,1)} copy(bf16[2048,2048]{0,1:T(8,128)(2,1)} %pad_maximum_fusion) | data formatting | bytes 16777216
  179.4 0.0 copy-start.3
  179.4 0.0 reduce-scatter.4.cloned.1.call-update
  179.4 13.4 %all-gather.8.cloned.1.call-done = bf16[2048,1024]{1,0:T(8,128)(2,1)} async-done(((bf16[128,1024]{1,0:T(8,128)(2,1)}), bf16[2048,1024]{1,0:T(8,128)(2,1)}) %all-gather.8.cloned.1.call-update) | async-done | bytes 4194320 | tf_op jit(solution)/shard_map/all_gather | solution.py:41
  192.8 0.0 copy-done.3
  192.8 9.3 %convolution_convert_fusion = bf16[1536,2048]{1,0:T(8,128)(2,1)S(1)} fusion(bf16[1536,1024]{1,0:T(8,128)(2,1)S(1)} %copy-done.3, bf16[2048,1024]{1,0:T(8,128)(2,1)} %all-gather.8.cloned.1.call-done), kind=kOutput, calls=%fused_computation.1 | convolution fusion | flops 6445596672 | bytes 13631488 | tf_op jit(solution)/shard_map/dot_general | solution.py:39
  202.2 76.1 %all_to_all.5 = bf16[8,192,2048]{2,1,0:T(8,128)(2,1)} all-to-all(bf16[8,192,2048]{2,1,0:T(8,128)(2,1)S(1)} %bitcast.8), channel_id=1, replica_groups=mesh['fs'=16,'tp'=8] {'tp'}, dimensions={0} | all-to-all | bytes 12582912 | tf_op jit(solution)/shard_map/all_to_all | solution.py:23
  278.3 5.2 %reduce_sum.12 = bf16[192,2048]{1,0:T(8,128)(2,1)} reduce(bf16[8,192,2048]{2,1,0:T(8,128)(2,1)} %all_to_all.5, bf16[]{:T(256)} %constant.6.clone.1), dimensions={0}, to_apply=%region_0.0 | reduce | flops 2752512 | bytes 7077890 | tf_op jit(solution)/shard_map/reduce_sum | solution.py:24
  283.5 0.0 reduce-scatter.4.cloned.1.call-done
  283.5 1.3 copy.11
  284.8 0.1 convert_element_type.24
  284.9 0.8 slice_bitcast_fusion
  285.8 1.0 copy.9
  (1 shorter events, 0.0 us)
Async XLA Ops:
  7.2 73.8 %all-gather.4.cloned.1.call-start = ((), (), s32[]{:S(2)}) async-start(), calls=%async_computation.2 | async-start | bytes 14155776 | tf_op jit(solution)/shard_map/all_gather | solution.py:13
  9.9 128.8 %all-gather.6.cloned.1.call-start = ((), (), s32[]{:S(2)}) async-start(), calls=%async_computation.3 | async-start | bytes 4456448 | tf_op jit(solution)/shard_map/all_gather | solution.py:35
  10.7 182.1 %all-gather.8.cloned.1.call-start = ((), (), s32[]{:S(2)}) async-start(), calls=%async_computation.4 | async-start | bytes 4456448 | tf_op jit(solution)/shard_map/all_gather | solution.py:41
  11.4 127.3 %copy-start.1 = (bf16[1536,1024]{1,0:T(8,128)(2,1)S(1)}, bf16[1536,1024]{1,0:T(8,128)(2,1)}, u32[]{:S(2)}) copy-start(bf16[1536,1024]{1,0:T(8,128)(2,1)} %param.6) | copy-start | bytes 9437188
  11.4 272.0 %reduce-scatter.4.cloned.1.call-start = ((), (), s32[]{:S(2)}) async-start(), calls=%async_computation.5 | async-start | bytes 8912896
  138.7 12.0 %copy-start = (bf16[1536,4096]{1,0:T(8,128)(2,1)S(1)}, bf16[1536,4096]{1,0:T(8,128)(2,1)}, u32[]{:S(2)}) copy-start(bf16[1536,4096]{1,0:T(8,128)(2,1)} %all-gather.4.cloned.1.call-done) | copy-start | bytes 37748740
  149.0 1.7 copy-start.2
  179.4 13.4 %copy-start.3 = (bf16[1536,1024]{1,0:T(8,128)(2,1)S(1)}, bf16[1536,1024]{1,0:T(8,128)(2,1)}, u32[]{:S(2)}) copy-start(bf16[1536,1024]{1,0:T(8,128)(2,1)} %copy-done.2) | copy-start | bytes 9437188
Sparse Core Ops, SparseCore 0:
  10.1 70.8 all-gather.3
  83.0 55.6 all-gather.5
  140.8 51.9 all-gather.7
  196.1 84.5 reduce-scatter.3
where the time goes:
time: 294 us; the launch traced here: 293 us
  waiting for transfers between devices  130 us (44%)
  blocking collectives  76.1 us (26%)
  matrix products  39.6 us (13%)
  local copies, waits for them, and re-layouts  16.8 us (6%)
  other arithmetic  16.4 us (6%)
  between operations  13.8 us (5%)
    all_to_all x1, blocking collectives, sum_at_owner(): lax.all_to_all(tiles, axis, split_axis=0, concat_axis=0, tiled=True)  76.1 us
    all_gather x1, waiting for transfers between devices, sent_together(): lax.all_gather(both, axis, axis=dim, tiled=True)  69.5 us
    all_gather x1, waiting for transfers between devices, local(): lax.all_gather(down_weight, 'fs', axis=1, tiled=True)  46.1 us
    unnamed x11, local copies, waits for them, and re-layouts  15.9 us
    all_gather x1, waiting for transfers between devices, local(): lax.all_gather(up_weight, 'fs', axis=0, tiled=True)  13.4 us
    dot_general x1, matrix products, local(): jnp.dot(grad_rows.T, hidden, preferred_element_type=jnp.float32)  11.6 us
    dot_general x1, matrix products, local(): jnp.dot(columns, lax.all_gather(down_weight, 'fs', axis=1, tiled=True).T,...  10.3 us
    dot_general x1, matrix products, local(): jnp.dot(pre_grad, lax.all_gather(up_weight, 'fs', axis=0, tiled=True).T,...  9.33 us
  transfers between devices with their start and end apart: 4, of which 3 were waited for; matrix products, arithmetic and copies ran while one was open for 22% of the time, Pallas kernels for 0%

commit v1 on v0

--- a/solution.py
+++ b/solution.py
@@ -2,6 +2,24 @@
 import jax.numpy as jnp
 from jax import lax
 from jax.sharding import PartitionSpec as P
+
+
+def collect(value, axis, dim):
+    ways, here, step = (lax.axis_size(axis), lax.axis_index(axis), value.shape[dim])
+    shape = [n * ways if d == dim else n for d, n in enumerate(value.shape)]
+    full = lax.dynamic_update_slice_in_dim(
+        jnp.zeros(shape, value.dtype), value, here * step, axis=dim
+    )
+    going_up = going_down = value
+    for far in range(1, ways // 2 + 1):
+        going_up = lax.ppermute(going_up, axis, [(d, (d + 1) % ways) for d in range(ways)])
+        full = lax.dynamic_update_slice_in_dim(full, going_up, (here - far) % ways * step, axis=dim)
+        if 2 * far < ways:
+            going_down = lax.ppermute(going_down, axis, [(d, (d - 1) % ways) for d in range(ways)])
+            full = lax.dynamic_update_slice_in_dim(
+                full, going_down, (here + far) % ways * step, axis=dim
+            )
+    return full
 
 
 def sent_together(arrays, axis, dim, along):
@@ -31,9 +49,7 @@
     width = pre_act.shape[1]
     columns = grad_rows
     hidden_grad = jnp.dot(
-        columns,
-        lax.all_gather(down_weight, "fs", axis=1, tiled=True).T,
-        preferred_element_type=jnp.float32,
+        columns, collect(down_weight, "fs", 1).T, preferred_element_type=jnp.float32
     )
     pre_grad = (2.0 * active * hidden_grad).astype(jnp.bfloat16)
     partial_value = jnp.dot(

time: 294 us -> 249 us (0.85)
  waiting for transfers between devices: 130 us -> 25.2 us
  starting transfers between devices: 0.16 us -> 37.3 us
  local copies, waits for them, and re-layouts: 16.8 us -> 33.8 us
  blocking collectives: 76.1 us -> 83.4 us
    all_gather x1, waiting for transfers between devices: 69.5 us -> 0.01 us  [sent_together(): lax.all_gather(both, axis, axis=dim, tiled=True)]
    all_gather x1 -> x0, waiting for transfers between devices: 46.1 us -> none  [local(): lax.all_gather(down_weight, 'fs', axis=1, tiled=True)]
    ppermute x0 -> x15, starting transfers between devices: none -> 37.2 us  [the longest x7 35 us: collect(): lax.ppermute(going_down, axis, [(d, (d - 1) % ways) for d in range(ways)])]
    ppermute x0 -> x15, waiting for transfers between devices: none -> 25.2 us  [the longest x8 20.8 us: collect(): lax.ppermute(going_up, axis, [(d, (d + 1) % ways) for d in range(ways)])]
    all_gather x1, waiting for transfers between devices: 13.4 us -> 0.02 us  [local(): lax.all_gather(up_weight, 'fs', axis=0, tiled=True)]
    dynamic_update_slice x0 -> x16, local copies, waits for them, and re-layouts: none -> 12.3 us  [the longest x8 6.11 us: collect(): lax.dynamic_update_slice_in_dim(full, going_up, (here - far) % ways * ste...]
    all_to_all x1, blocking collectives: 76.1 us -> 83.4 us  [sum_at_owner(): lax.all_to_all(tiles, axis, split_axis=0, concat_axis=0, tiled=True)]
    unnamed x11 -> x13, local copies, waits for them, and re-layouts: 15.9 us -> 18.2 us
  transfers between devices with their start and end apart: 4 -> 18, of which waited for: 3 -> 8; matrix products, arithmetic and copies ran while one was open for 22% -> 32% of each run, Pallas kernels for 0% -> 0%
where the time goes in v1:
time: 249 us; the launch traced here: 248 us
  blocking collectives  83.4 us (33%)
  matrix products  38.5 us (15%)
  starting transfers between devices  37.3 us (15%)
  local copies, waits for them, and re-layouts  33.8 us (14%)
  waiting for transfers between devices  25.2 us (10%)
  other arithmetic  16.4 us (7%)
  between operations  13.9 us (6%)
    all_to_all x1, blocking collectives, sum_at_owner(): lax.all_to_all(tiles, axis, split_axis=0, concat_axis=0, tiled=True)  83.4 us
    ppermute x7, starting transfers between devices, collect(): lax.ppermute(going_down, axis, [(d, (d - 1) % ways) for d in range(ways)])  35 us
    ppermute x8, waiting for transfers between devices, collect(): lax.ppermute(going_up, axis, [(d, (d + 1) % ways) for d in range(ways)])  20.8 us
    unnamed x13, local copies, waits for them, and re-layouts  18.2 us
    dot_general x1, matrix products, local(): jnp.dot(grad_rows.T, hidden, preferred_element_type=jnp.float32)  11.8 us
    dot_general x1, matrix products, local(): jnp.dot(pre_grad, lax.all_gather(up_weight, 'fs', axis=0, tiled=True).T,...  9.32 us
    dot_general x1, matrix products, local(): jnp.dot(columns, collect(down_weight, 'fs', 1).T, preferred_element_type=...  8.99 us
    concatenate x1, other arithmetic, local(): jnp.concatenate([jnp.dot(columns.T, pre_grad, preferred_element_type=jnp....  8.48 us
  transfers between devices with their start and end apart: 18, of which 8 were waited for; matrix products, arithmetic and copies ran while one was open for 32% of the time, Pallas kernels for 0%

profile of v1, /device:TPU:1, one launch (start us, length us, event | category | flops | bytes accessed | tf_op | source)
XLA Modules:
  0.0 248.5 jit_solution(15034942445907817228)
XLA Ops:
  7.2 0.0 all-gather.3.cloned.1.call-start
  7.2 2.7 %pad_maximum_fusion.1 = bf16[192,4096]{1,0:T(8,128)(2,1)} fusion(bf16[192,2048]{1,0:T(8,128)(2,1)} %param.7, bf16[192,2048]{1,0:T(8,128)(2,1)} %param.5), kind=kLoop, calls=%fused_computation.14 | loop fusion | flops 3145728 | bytes 3145728 | tf_op jit(solution)/shard_map/concatenate | solution.py:30
  10.0 0.0 all-gather.3.cloned.1.call-update
  10.0 0.0 all-gather.5.cloned.1.call-start
  10.0 2.2 collective-permute-start
  12.2 5.0 %collective-permute-start.1 = (bf16[1024,128]{1,0:T(8,128)(2,1)S(1)}, bf16[1024,128]{1,0:T(8,128)(2,1)S(1)}, u32[]{:S(2)}, u32[]{:S(2)}) collective-permute-start(bf16[1024,128]{1,0:T(8,128)(2,1)S(1)} %copy-done), channel_id=1, source_target_pairs={{0,120},{8,0},{16,8},{24,16},{32,24},{40,32},{48,40},{56,48},{64,5... | collective-permute-start | bytes 786440 | tf_op jit(solution)/shard_map/ppermute | solution.py:18
  17.2 5.9 %collective-permute-done = bf16[1024,128]{1,0:T(8,128)(2,1)S(1)} collective-permute-done((bf16[1024,128]{1,0:T(8,128)(2,1)S(1)}, bf16[1024,128]{1,0:T(8,128)(2,1)S(1)}, u32[]{:S(2)}, u32[]{:S(2)}) %collective-permute-start) | collective-permute-done | bytes 262176 | tf_op jit(solution)/shard_map/ppermute | solution.py:15
  23.2 0.0 collective-permute-start.2
  23.2 0.0 collective-permute-done.1
  23.2 4.8 %collective-permute-start.3 = (bf16[1024,128]{1,0:T(8,128)(2,1)S(1)}, bf16[1024,128]{1,0:T(8,128)(2,1)S(1)}, u32[]{:S(2)}, u32[]{:S(2)}) collective-permute-start(bf16[1024,128]{1,0:T(8,128)(2,1)S(1)} %collective-permute-done.1), channel_id=1, source_target_pairs={{0,120},{8,0},{16,8},{24,16},{32,24},{40,32},{48,40},{56,48},{64,5... | collective-permute-start | bytes 786440 | tf_op jit(solution)/shard_map/ppermute | solution.py:18
  27.9 5.1 %collective-permute-done.2 = bf16[1024,128]{1,0:T(8,128)(2,1)S(1)} collective-permute-done((bf16[1024,128]{1,0:T(8,128)(2,1)S(1)}, bf16[1024,128]{1,0:T(8,128)(2,1)S(1)}, u32[]{:S(2)}, u32[]{:S(2)}) %collective-permute-start.2) | collective-permute-done | bytes 262176 | tf_op jit(solution)/shard_map/ppermute | solution.py:15
  33.1 0.0 collective-permute-start.4
  33.1 0.0 collective-permute-done.3
  33.1 4.8 %collective-permute-start.5 = (bf16[1024,128]{1,0:T(8,128)(2,1)S(1)}, bf16[1024,128]{1,0:T(8,128)(2,1)S(1)}, u32[]{:S(2)}, u32[]{:S(2)}) collective-permute-start(bf16[1024,128]{1,0:T(8,128)(2,1)S(1)} %collective-permute-done.3), channel_id=1, source_target_pairs={{0,120},{8,0},{16,8},{24,16},{32,24},{40,32},{48,40},{56,48},{64,5... | collective-permute-start | bytes 786440 | tf_op jit(solution)/shard_map/ppermute | solution.py:18
  37.9 0.0 all-gather.5.cloned.1.call-update
  37.9 0.0 reduce-scatter.4.cloned.1.call-start
  38.0 4.2 %collective-permute-done.4 = bf16[1024,128]{1,0:T(8,128)(2,1)S(1)} collective-permute-done((bf16[1024,128]{1,0:T(8,128)(2,1)S(1)}, bf16[1024,128]{1,0:T(8,128)(2,1)S(1)}, u32[]{:S(2)}, u32[]{:S(2)}) %collective-permute-start.4) | collective-permute-done | bytes 262176 | tf_op jit(solution)/shard_map/ppermute | solution.py:15
  42.2 0.0 collective-permute-start.6
  42.2 2.5 broadcast_in_dim.3
  44.6 0.8 constant_dynamic-update-slice_fusion.15
  45.4 0.8 constant_dynamic-update-slice_fusion.14
  46.2 0.0 collective-permute-done.5
  46.2 4.8 %collective-permute-start.7 = (bf16[1024,128]{1,0:T(8,128)(2,1)S(1)}, bf16[1024,128]{1,0:T(8,128)(2,1)S(1)}, u32[]{:S(2)}, u32[]{:S(2)}) collective-permute-start(bf16[1024,128]{1,0:T(8,128)(2,1)S(1)} %collective-permute-done.5), channel_id=1, source_target_pairs={{0,120},{8,0},{16,8},{24,16},{32,24},{40,32},{48,40},{56,48},{64,5... | collective-permute-start | bytes 786440 | tf_op jit(solution)/shard_map/ppermute | solution.py:18
  50.9 0.8 constant_dynamic-update-slice_fusion.13
  51.7 0.8 constant_dynamic-update-slice_fusion.12
  52.5 0.8 constant_dynamic-update-slice_fusion.11
  53.2 1.0 collective-permute-done.7
  54.3 5.2 %collective-permute-start.9 = (bf16[1024,128]{1,0:T(8,128)(2,1)S(1)}, bf16[1024,128]{1,0:T(8,128)(2,1)S(1)}, u32[]{:S(2)}, u32[]{:S(2)}) collective-permute-start(bf16[1024,128]{1,0:T(8,128)(2,1)S(1)} %collective-permute-done.7), channel_id=1, source_target_pairs={{0,120},{8,0},{16,8},{24,16},{32,24},{40,32},{48,40},{56,48},{64,5... | collective-permute-start | bytes 786440 | tf_op jit(solution)/shard_map/ppermute | solution.py:18
  59.5 0.8 constant_dynamic-update-slice_fusion.10
  60.3 0.7 constant_dynamic-update-slice_fusion.9
  61.0 0.7 constant_dynamic-update-slice_fusion.8
  61.8 1.0 collective-permute-done.9
  62.8 5.2 %collective-permute-start.11 = (bf16[1024,128]{1,0:T(8,128)(2,1)S(1)}, bf16[1024,128]{1,0:T(8,128)(2,1)S(1)}, u32[]{:S(2)}, u32[]{:S(2)}) collective-permute-start(bf16[1024,128]{1,0:T(8,128)(2,1)S(1)} %collective-permute-done.9), channel_id=1, source_target_pairs={{0,120},{8,0},{16,8},{24,16},{32,24},{40,32},{48,40},{56,48},{64,5... | collective-permute-start | bytes 786440 | tf_op jit(solution)/shard_map/ppermute | solution.py:18
  68.0 0.8 constant_dynamic-update-slice_fusion.7
  68.8 0.0 collective-permute-done.10
  68.8 0.8 constant_dynamic-update-slice_fusion.6
  69.6 0.8 constant_dynamic-update-slice_fusion.5
  70.4 1.0 collective-permute-done.11
  71.3 5.2 %collective-permute-start.13 = (bf16[1024,128]{1,0:T(8,128)(2,1)S(1)}, bf16[1024,128]{1,0:T(8,128)(2,1)S(1)}, u32[]{:S(2)}, u32[]{:S(2)}) collective-permute-start(bf16[1024,128]{1,0:T(8,128)(2,1)S(1)} %collective-permute-done.11), channel_id=1, source_target_pairs={{0,120},{8,0},{16,8},{24,16},{32,24},{40,32},{48,40},{56,48},{64,5... | collective-permute-start | bytes 786440 | tf_op jit(solution)/shard_map/ppermute | solution.py:18
  76.6 0.8 constant_dynamic-update-slice_fusion.4
  77.3 0.0 collective-permute-done.12
  77.4 0.0 collective-permute-start.14
  77.4 0.8 constant_dynamic-update-slice_fusion.3
  78.2 0.7 constant_dynamic-update-slice_fusion.2
  78.9 1.3 collective-permute-done.13
  80.2 0.8 constant_dynamic-update-slice_fusion.1
  80.9 5.5 %collective-permute-done.14 = bf16[1024,128]{1,0:T(8,128)(2,1)S(1)} collective-permute-done((bf16[1024,128]{1,0:T(8,128)(2,1)S(1)}, bf16[1024,128]{1,0:T(8,128)(2,1)S(1)}, u32[]{:S(2)}, u32[]{:S(2)}) %collective-permute-start.14) | collective-permute-done | bytes 262176 | tf_op jit(solution)/shard_map/ppermute | solution.py:15
  86.4 0.8 constant_dynamic-update-slice_fusion
  87.3 11.8 %fusion.8 = bf16[2048,1024]{0,1:T(8,128)(2,1)} fusion(bf16[1536,4096]{1,0:T(8,128)(2,1)} %all-gather.3.cloned.1.call-done, bf16[1536,1024]{1,0:T(8,128)(2,1)} %param.6), kind=kOutput, calls=%fused_computation.11 | convolution fusion | flops 6450839552 | bytes 13631488 | tf_op jit(solution)/shard_map/dot_general | solution.py:68
  99.1 9.0 %multiply_convert_fusion.1 = bf16[1536,1024]{1,0:T(8,128)(2,1)S(1)} fusion(bf16[1536,1024]{1,0:T(8,128)(2,1)S(1)} %copy-done.2, bf16[1024,2048]{1,0:T(8,128)(2,1)} %constant_dynamic-update-slice_fusion, bf16[1536,4096]{1,0:T(8,128)(2,1)S(1)} %copy-done.1), kind=kOutput, calls=%fused_computation.5 | convolution fusion | flops 6450315264 | bytes 16777216 | tf_op jit(solution)/shard_map/dot_general | solution.py:51
  108.1 1.7 copy-done.3
  109.8 8.4 %fusion.11 = bf16[2048,1024]{0,1:T(8,128)(2,1)} fusion(bf16[1536,1024]{1,0:T(8,128)(2,1)S(1)} %multiply_convert_fusion.1, bf16[1536,4096]{1,0:T(8,128)(2,1)S(1)} %copy-done.1), kind=kOutput, calls=%fused_computation.12 | convolution fusion | flops 6444548096 | bytes 13631488 | tf_op jit(solution)/shard_map/dot_general | solution.py:67
  118.1 8.5 %pad_maximum_fusion = bf16[2048,2048]{0,1:T(8,128)(2,1)} fusion(bf16[2048,1024]{0,1:T(8,128)(2,1)} %fusion.8, bf16[2048,1024]{0,1:T(8,128)(2,1)} %fusion.11), kind=kLoop, calls=%fused_computation | loop fusion | flops 16777216 | bytes 16777216 | tf_op jit(solution)/shard_map/concatenate | solution.py:65
  126.6 12.4 %copy.10 = bf16[2048,2048]{1,0:T(8,128)(2,1)} copy(bf16[2048,2048]{0,1:T(8,128)(2,1)} %pad_maximum_fusion) | data formatting | bytes 16777216
  139.0 0.0 reduce-scatter.4.cloned.1.call-update
  139.0 0.0 all-gather.5.cloned.1.call-done
  139.0 1.8 copy-done.4
  140.9 9.3 %convolution_convert_fusion = bf16[1536,2048]{1,0:T(8,128)(2,1)S(1)} fusion(bf16[1536,1024]{1,0:T(8,128)(2,1)S(1)} %copy-done.4, bf16[2048,1024]{1,0:T(8,128)(2,1)} %all-gather.5.cloned.1.call-done), kind=kOutput, calls=%fused_computation.1 | convolution fusion | flops 6445596672 | bytes 13631488 | tf_op jit(solution)/shard_map/dot_general | solution.py:55
  150.2 83.4 %all_to_all.5 = bf16[8,192,2048]{2,1,0:T(8,128)(2,1)} all-to-all(bf16[8,192,2048]{2,1,0:T(8,128)(2,1)S(1)} %bitcast.8), channel_id=1, replica_groups=mesh['fs'=16,'tp'=8] {'tp'}, dimensions={0} | all-to-all | bytes 12582912 | tf_op jit(solution)/shard_map/all_to_all | solution.py:41
  233.6 5.1 %reduce_sum.12 = bf16[192,2048]{1,0:T(8,128)(2,1)} reduce(bf16[8,192,2048]{2,1,0:T(8,128)(2,1)} %all_to_all.5, bf16[]{:T(256)} %constant.96.clone.1), dimensions={0}, to_apply=%region_0.1 | reduce | flops 2752512 | bytes 7077890 | tf_op jit(solution)/shard_map/reduce_sum | solution.py:42
  238.7 1.3 copy.11
  240.0 0.1 convert_element_type.24
  240.1 0.8 slice_bitcast_fusion
  241.0 1.0 copy.9
  (16 shorter events, 0.1 us)
Async XLA Ops:
  7.2 2.9 %copy-start = (bf16[1024,128]{1,0:T(8,128)(2,1)S(1)}, bf16[1024,128]{1,0:T(8,128)(2,1)}, u32[]{:S(2)}) copy-start(bf16[1024,128]{1,0:T(8,128)(2,1)} %param.9) | copy-start | bytes 786436
  7.2 80.1 %all-gather.3.cloned.1.call-start = ((), (), s32[]{:S(2)}) async-start(), calls=%async_computation.2 | async-start | bytes 14155776 | tf_op jit(solution)/shard_map/all_gather | solution.py:31
  10.0 129.0 %all-gather.5.cloned.1.call-start = ((), (), s32[]{:S(2)}) async-start(), calls=%async_computation.3 | async-start | bytes 4456448 | tf_op jit(solution)/shard_map/all_gather | solution.py:57
  10.0 13.1 %collective-permute-start = (bf16[1024,128]{1,0:T(8,128)(2,1)S(1)}, bf16[1024,128]{1,0:T(8,128)(2,1)S(1)}, u32[]{:S(2)}, u32[]{:S(2)}) collective-permute-start(bf16[1024,128]{1,0:T(8,128)(2,1)S(1)} %copy-done), channel_id=1, source_target_pairs={{0,8},{8,16},{16,24},{24,32},{32,40},{40,48},{48,56},{56,64},{64,7... | collective-permute-start | bytes 786440 | tf_op jit(solution)/shard_map/ppermute | solution.py:15
  12.2 10.9 %collective-permute-start.1 = (bf16[1024,128]{1,0:T(8,128)(2,1)S(1)}, bf16[1024,128]{1,0:T(8,128)(2,1)S(1)}, u32[]{:S(2)}, u32[]{:S(2)}) collective-permute-start(bf16[1024,128]{1,0:T(8,128)(2,1)S(1)} %copy-done), channel_id=1, source_target_pairs={{0,120},{8,0},{16,8},{24,16},{32,24},{40,32},{48,40},{56,48},{64,5... | collective-permute-start | bytes 786440 | tf_op jit(solution)/shard_map/ppermute | solution.py:18
  23.2 9.9 %collective-permute-start.2 = (bf16[1024,128]{1,0:T(8,128)(2,1)S(1)}, bf16[1024,128]{1,0:T(8,128)(2,1)S(1)}, u32[]{:S(2)}, u32[]{:S(2)}) collective-permute-start(bf16[1024,128]{1,0:T(8,128)(2,1)S(1)} %collective-permute-done), channel_id=1, source_target_pairs={{0,8},{8,16},{16,24},{24,32},{32,40},{40,48},{48,56},{56,64},{64,7... | collective-permute-start | bytes 786440 | tf_op jit(solution)/shard_map/ppermute | solution.py:15
  23.2 9.9 %collective-permute-start.3 = (bf16[1024,128]{1,0:T(8,128)(2,1)S(1)}, bf16[1024,128]{1,0:T(8,128)(2,1)S(1)}, u32[]{:S(2)}, u32[]{:S(2)}) collective-permute-start(bf16[1024,128]{1,0:T(8,128)(2,1)S(1)} %collective-permute-done.1), channel_id=1, source_target_pairs={{0,120},{8,0},{16,8},{24,16},{32,24},{40,32},{48,40},{56,48},{64,5... | collective-permute-start | bytes 786440 | tf_op jit(solution)/shard_map/ppermute | solution.py:18
  33.1 9.1 %collective-permute-start.4 = (bf16[1024,128]{1,0:T(8,128)(2,1)S(1)}, bf16[1024,128]{1,0:T(8,128)(2,1)S(1)}, u32[]{:S(2)}, u32[]{:S(2)}) collective-permute-start(bf16[1024,128]{1,0:T(8,128)(2,1)S(1)} %collective-permute-done.2), channel_id=1, source_target_pairs={{0,8},{8,16},{16,24},{24,32},{32,40},{40,48},{48,56},{56,64},{64,7... | collective-permute-start | bytes 786440 | tf_op jit(solution)/shard_map/ppermute | solution.py:15
  33.1 13.1 %collective-permute-start.5 = (bf16[1024,128]{1,0:T(8,128)(2,1)S(1)}, bf16[1024,128]{1,0:T(8,128)(2,1)S(1)}, u32[]{:S(2)}, u32[]{:S(2)}) collective-permute-start(bf16[1024,128]{1,0:T(8,128)(2,1)S(1)} %collective-permute-done.3), channel_id=1, source_target_pairs={{0,120},{8,0},{16,8},{24,16},{32,24},{40,32},{48,40},{56,48},{64,5... | collective-permute-start | bytes 786440 | tf_op jit(solution)/shard_map/ppermute | solution.py:18
  37.9 200.8 %reduce-scatter.4.cloned.1.call-start = ((), (), s32[]{:S(2)}) async-start(), calls=%async_computation.4 | async-start | bytes 8912896
  42.2 9.5 %collective-permute-start.6 = (bf16[1024,128]{1,0:T(8,128)(2,1)S(1)}, bf16[1024,128]{1,0:T(8,128)(2,1)S(1)}, u32[]{:S(2)}, u32[]{:S(2)}) collective-permute-start(bf16[1024,128]{1,0:T(8,128)(2,1)S(1)} %collective-permute-done.4), channel_id=1, source_target_pairs={{0,8},{8,16},{16,24},{24,32},{32,40},{40,48},{48,56},{56,64},{64,7... | collective-permute-start | bytes 786440 | tf_op jit(solution)/shard_map/ppermute | solution.py:15
  46.2 8.1 %collective-permute-start.7 = (bf16[1024,128]{1,0:T(8,128)(2,1)S(1)}, bf16[1024,128]{1,0:T(8,128)(2,1)S(1)}, u32[]{:S(2)}, u32[]{:S(2)}) collective-permute-start(bf16[1024,128]{1,0:T(8,128)(2,1)S(1)} %collective-permute-done.5), channel_id=1, source_target_pairs={{0,120},{8,0},{16,8},{24,16},{32,24},{40,32},{48,40},{56,48},{64,5... | collective-permute-start | bytes 786440 | tf_op jit(solution)/shard_map/ppermute | solution.py:18
  51.7 8.6 %collective-permute-start.8 = (bf16[1024,128]{1,0:T(8,128)(2,1)S(1)}, bf16[1024,128]{1,0:T(8,128)(2,1)S(1)}, u32[]{:S(2)}, u32[]{:S(2)}) collective-permute-start(bf16[1024,128]{1,0:T(8,128)(2,1)S(1)} %collective-permute-done.6), channel_id=1, source_target_pairs={{0,8},{8,16},{16,24},{24,32},{32,40},{40,48},{48,56},{56,64},{64,7... | collective-permute-start | bytes 786440 | tf_op jit(solution)/shard_map/ppermute | solution.py:15
  54.3 8.5 %collective-permute-start.9 = (bf16[1024,128]{1,0:T(8,128)(2,1)S(1)}, bf16[1024,128]{1,0:T(8,128)(2,1)S(1)}, u32[]{:S(2)}, u32[]{:S(2)}) collective-permute-start(bf16[1024,128]{1,0:T(8,128)(2,1)S(1)} %collective-permute-done.7), channel_id=1, source_target_pairs={{0,120},{8,0},{16,8},{24,16},{32,24},{40,32},{48,40},{56,48},{64,5... | collective-permute-start | bytes 786440 | tf_op jit(solution)/shard_map/ppermute | solution.py:18
  60.3 8.5 %collective-permute-start.10 = (bf16[1024,128]{1,0:T(8,128)(2,1)S(1)}, bf16[1024,128]{1,0:T(8,128)(2,1)S(1)}, u32[]{:S(2)}, u32[]{:S(2)}) collective-permute-start(bf16[1024,128]{1,0:T(8,128)(2,1)S(1)} %collective-permute-done.8), channel_id=1, source_target_pairs={{0,8},{8,16},{16,24},{24,32},{32,40},{40,48},{48,56},{56,64},{64,7... | collective-permute-start | bytes 786440 | tf_op jit(solution)/shard_map/ppermute | solution.py:15
  62.8 8.5 %collective-permute-start.11 = (bf16[1024,128]{1,0:T(8,128)(2,1)S(1)}, bf16[1024,128]{1,0:T(8,128)(2,1)S(1)}, u32[]{:S(2)}, u32[]{:S(2)}) collective-permute-start(bf16[1024,128]{1,0:T(8,128)(2,1)S(1)} %collective-permute-done.9), channel_id=1, source_target_pairs={{0,120},{8,0},{16,8},{24,16},{32,24},{40,32},{48,40},{56,48},{64,5... | collective-permute-start | bytes 786440 | tf_op jit(solution)/shard_map/ppermute | solution.py:18
  68.8 8.5 %collective-permute-start.12 = (bf16[1024,128]{1,0:T(8,128)(2,1)S(1)}, bf16[1024,128]{1,0:T(8,128)(2,1)S(1)}, u32[]{:S(2)}, u32[]{:S(2)}) collective-permute-start(bf16[1024,128]{1,0:T(8,128)(2,1)S(1)} %collective-permute-done.10), channel_id=1, source_target_pairs={{0,8},{8,16},{16,24},{24,32},{32,40},{40,48},{48,56},{56,64},{64,7... | collective-permute-start | bytes 786440 | tf_op jit(solution)/shard_map/ppermute | solution.py:15
  71.3 8.8 %collective-permute-start.13 = (bf16[1024,128]{1,0:T(8,128)(2,1)S(1)}, bf16[1024,128]{1,0:T(8,128)(2,1)S(1)}, u32[]{:S(2)}, u32[]{:S(2)}) collective-permute-start(bf16[1024,128]{1,0:T(8,128)(2,1)S(1)} %collective-permute-done.11), channel_id=1, source_target_pairs={{0,120},{8,0},{16,8},{24,16},{32,24},{40,32},{48,40},{56,48},{64,5... | collective-permute-start | bytes 786440 | tf_op jit(solution)/shard_map/ppermute | solution.py:18
  77.4 9.1 %collective-permute-start.14 = (bf16[1024,128]{1,0:T(8,128)(2,1)S(1)}, bf16[1024,128]{1,0:T(8,128)(2,1)S(1)}, u32[]{:S(2)}, u32[]{:S(2)}) collective-permute-start(bf16[1024,128]{1,0:T(8,128)(2,1)S(1)} %collective-permute-done.12), channel_id=1, source_target_pairs={{0,8},{8,16},{16,24},{24,32},{32,40},{40,48},{48,56},{56,64},{64,7... | collective-permute-start | bytes 786440 | tf_op jit(solution)/shard_map/ppermute | solution.py:15
  87.2 11.8 %copy-start.2 = (bf16[1536,1024]{1,0:T(8,128)(2,1)S(1)}, bf16[1536,1024]{1,0:T(8,128)(2,1)}, u32[]{:S(2)}) copy-start(bf16[1536,1024]{1,0:T(8,128)(2,1)} %param.6) | copy-start | bytes 9437188
  87.2 11.8 %copy-start.1 = (bf16[1536,4096]{1,0:T(8,128)(2,1)S(1)}, bf16[1536,4096]{1,0:T(8,128)(2,1)}, u32[]{:S(2)}) copy-start(bf16[1536,4096]{1,0:T(8,128)(2,1)} %all-gather.3.cloned.1.call-done) | copy-start | bytes 37748740
  108.1 1.7 copy-start.3
  139.0 1.9 copy-start.4
Sparse Core Ops, SparseCore 0:
  10.1 70.8 all-gather.2
  83.1 51.3 all-gather.4
  139.1 88.4 reduce-scatter.3
